TPU v7x, 128 devices: a whole 4x4x4 slice. The times are simulated.
128 devices in a mesh: ep: 32 (over z, y, core), tp: 4 (over x).
Axes of the slice: x: 4, y: 4, z: 4, core: 2. Of those that a mesh axis runs over, the one named last changes fastest.
Arguments:
- gate_outer: bfloat16 [65536, 1024], P(('ep', 'tp')), may hold values from -6 to 6
- gate_inner: bfloat16 [65536, 1024], P(('ep', 'tp')), may hold values from -6 to 6
- conv_input: bfloat16 [65536, 1024], P(('ep', 'tp')), may hold values from -6 to 6
- conv_taps: float32 [3, 1024], replicated, may hold values from -3.5 to 3.5
- mixer_out_weight: bfloat16 [1024, 2048], replicated, may hold values from -0.1875 to 0.1875
- moe_tokens: bfloat16 [16384, 2048], P(('ep', 'tp')), may hold values from -40 to 40
- norm_gain: float32 [2048], replicated, may hold values from 0.1 to 1.9
- expert_ids: int32 [16384, 4], P(('ep', 'tp')), may hold values from 0 to 127, all different within a row; in each aligned block of 128 rows (0 to 127, 128 to 255, ...) at most 6 rows name the same one
- route_weight: float32 [16384, 4], P(('ep', 'tp')), may hold values from 0.2 to 1
- expert_gate: bfloat16 [128, 2048, 1024], P(('ep', 'tp')), may hold values from -0.39648438 to 0.39648438
- expert_up: bfloat16 [128, 2048, 1024], P(('ep', 'tp')), may hold values from -0.39648438 to 0.39648438
- expert_down: bfloat16 [128, 1024, 2048], P(('ep', 'tp')), may hold values from -0.03125 to 0.03125
Outputs:
- mixed_out: bfloat16 [65536, 2048], P(('ep', 'tp'))
- moe_out: bfloat16 [16384, 2048], P(('ep', 'tp'))
Inputs may be any that keep to these rules, and one draw needn't show every extreme that they name: `expert_ids`: each token names 4 different experts. Among the tokens of one device no expert is named by more than 6 of them, and on some device an expert is named by exactly 6.
All inputs are finite; a program needn't handle non-finite values.
Results may differ from a plain program's by a relative error of at most 0.007.
Values may be sent and summed in bfloat16 or wider, within the bound.
A program may use at most 128 MiB of HBM per device.

v0:
```python
import jax
import jax.numpy as jnp
from jax import lax
from jax.sharding import PartitionSpec as P

epsilon = 1e-06
clamp_limit = 7.0
alpha_gate = 1.702


def from_behind(value, axis, by):
    length = lax.axis_size(axis)
    pairs = [(i, i + by) for i in range(length) if 0 <= i + by < length]
    return lax.ppermute(value, axis, pairs)


def expert_rows(row_block, gate_weight, up_weight, down_weight):
    gate_pre = jnp.dot(row_block, gate_weight, preferred_element_type=jnp.float32)
    up_pre = jnp.dot(row_block, up_weight, preferred_element_type=jnp.float32)
    gate_pre = jnp.minimum(gate_pre, clamp_limit)
    up_pre = jnp.clip(up_pre, -clamp_limit, clamp_limit)
    hidden = ((up_pre + 1.0) * (gate_pre * jax.nn.sigmoid(alpha_gate * gate_pre))).astype(
        jnp.bfloat16
    )
    return jnp.dot(hidden, down_weight, preferred_element_type=jnp.float32).astype(jnp.bfloat16)


def shards(
    gate_outer,
    gate_inner,
    conv_input,
    conv_taps,
    mixer_out_weight,
    moe_tokens,
    norm_gain,
    expert_ids,
    route_weight,
    expert_gate,
    expert_up,
    expert_down,
):
    reach_rows = conv_taps.shape[0] - 1
    rows_here = gate_inner.shape[0]
    product = (gate_inner.astype(jnp.float32) * conv_input.astype(jnp.float32)).astype(jnp.bfloat16)
    previous = from_behind(product[rows_here - reach_rows :], ("ep", "tp"), 1)
    extended = jnp.concatenate([previous, product], 0).astype(jnp.float32)
    convolved = jnp.zeros(product.shape, jnp.float32)
    for offset in range(conv_taps.shape[0]):
        convolved = convolved + conv_taps[offset][None, :] * extended[offset : offset + rows_here]
    gated_rows = (gate_outer.astype(jnp.float32) * convolved).astype(jnp.bfloat16)
    mixed_out = jnp.dot(gated_rows, mixer_out_weight, preferred_element_type=jnp.float32).astype(
        jnp.bfloat16
    )
    tokens_here = moe_tokens.shape[0]
    width = moe_tokens.shape[1]
    top_count = expert_ids.shape[1]
    experts_all = lax.axis_size("ep") * lax.axis_size("tp")
    capacity = 3 * tokens_here * top_count // (2 * experts_all)
    widened = moe_tokens.astype(jnp.float32)
    normed = (
        widened
        * lax.rsqrt(jnp.mean(widened * widened, axis=-1, keepdims=True) + epsilon)
        * norm_gain[None, :]
    ).astype(jnp.bfloat16)
    mix_weight = route_weight / jnp.sum(route_weight, axis=-1, keepdims=True)
    flat_ids = expert_ids.reshape(-1)
    one_hot = (flat_ids[:, None] == jnp.arange(experts_all, dtype=jnp.int32)[None, :]).astype(
        jnp.int32
    )
    earlier = jnp.cumsum(one_hot, axis=0) - one_hot
    slot_rank = jnp.sum(earlier * one_hot, axis=1)
    slot_index = (flat_ids * capacity + slot_rank).reshape(tokens_here, top_count)
    slot_range = jnp.arange(experts_all * capacity, dtype=jnp.int32)
    dispatch = jnp.any(slot_index[None, :, :] == slot_range[:, None, None], axis=2).astype(
        jnp.bfloat16
    )
    send_rows = jnp.dot(dispatch, normed, preferred_element_type=jnp.float32).astype(jnp.bfloat16)
    send_rows = send_rows.reshape(experts_all, capacity, width)
    received = lax.all_to_all(send_rows, ("ep", "tp"), split_axis=0, concat_axis=0, tiled=True)
    row_block = received.reshape(-1, width)
    expert_out = expert_rows(row_block, expert_gate[0], expert_up[0], expert_down[0])
    returned = lax.all_to_all(
        expert_out.reshape(received.shape), ("ep", "tp"), split_axis=0, concat_axis=0, tiled=True
    )
    flat_rows = returned.reshape(experts_all * capacity, width)
    picked = (
        flat_rows[slot_index.reshape(-1)].astype(jnp.float32).reshape(tokens_here, top_count, width)
    )
    moe_out = jnp.sum(picked * mix_weight[:, :, None], axis=1).astype(jnp.bfloat16)
    return (mixed_out, moe_out)


def solution(mesh):
    in_specs = (
        P(("ep", "tp"), None),
        P(("ep", "tp"), None),
        P(("ep", "tp"), None),
        P(),
        P(),
        P(("ep", "tp"), None),
        P(),
        P(("ep", "tp"), None),
        P(("ep", "tp"), None),
        P(("ep", "tp"), None, None),
        P(("ep", "tp"), None, None),
        P(("ep", "tp"), None, None),
    )
    out_specs = (P(("ep", "tp"), None), P(("ep", "tp"), None))
    return jax.shard_map(shards, mesh=mesh, in_specs=in_specs, out_specs=out_specs, check_vma=False)
```

profile of v0, /device:TPU:1, one launch (start us, length us, event | category | flops | bytes accessed | tf_op | source)
XLA Modules:
  0.0 172.4 jit_solution(3247060331957236064)
XLA Ops:
  0.6 0.8 copy.22
  1.4 0.1 eq.42
  1.5 0.1 eq.38
  1.6 0.1 copy.25
  1.7 0.2 fusion.28
  2.1 0.2 fusion.27
  2.3 0.1 reduce_sum.41
  2.4 0.1 copy.27
  2.5 0.2 fusion.15
  2.7 1.2 fusion.16
  4.0 2.1 %convolution_convert_fusion = bf16[768,2048]{1,0:T(8,128)(2,1)S(1)} fusion(pred[768,128]{1,0:T(8,128)(4,1)S(1)} %fusion.15, bf16[128,2048]{1,0:T(8,128)(2,1)} %param.17, f32[2048]{0:T(1024)} %param.18, f32[128]{0:T(128)S(1)} %add_rsqrt_fusion), kind=kOutput, calls=%fused_computation.9 | convolution fusion | flops 405274624 | bytes 3777024 | tf_op jit(solution)/shard_map/dot_general | solution.py:77
  6.1 2.9 %reshape.84 = bf16[128,6,2048]{2,1,0:T(8,128)(2,1)} reshape(bf16[768,2048]{1,0:T(8,128)(2,1)S(1)} %convolution_convert_fusion) | data formatting | bytes 6291456 | tf_op jit(solution)/shard_map/reshape | solution.py:78
  9.0 65.0 %all_to_all.10 = bf16[128,6,2048]{2,1,0:T(8,128)(2,1)} all-to-all(bf16[128,6,2048]{2,1,0:T(8,128)(2,1)} %reshape.84), channel_id=1, replica_groups=mesh['ep'=32,'tp'=4] {'ep','tp'}, dimensions={0} | all-to-all | bytes 6291456 | tf_op jit(solution)/shard_map/all_to_all | solution.py:79
  73.9 4.9 %reshape.85 = bf16[768,2048]{1,0:T(8,128)(2,1)S(1)} reshape(bf16[128,6,2048]{2,1,0:T(8,128)(2,1)} %all_to_all.10) | data formatting | bytes 6291456 | tf_op jit(solution)/shard_map/reshape | solution.py:80
  78.8 0.0 copy-start.4
  78.8 5.4 %fusion.2 = f32[768,1024]{1,0:T(8,128)S(1)} fusion(bf16[768,2048]{1,0:T(8,128)(2,1)S(1)} %reshape.85, bf16[1,2048,1024]{2,1,0:T(8,128)(2,1)} %param.21), kind=kOutput, calls=%fused_computation.3 | convolution fusion | flops 3221225472 | bytes 10485760 | tf_op jit(solution)/shard_map/dot_general | solution.py:18
  84.2 0.0 copy-done.4
  84.2 0.0 copy-start.5
  84.2 4.0 %multiply_convert_fusion = bf16[768,1024]{1,0:T(8,128)(2,1)S(1)} fusion(f32[768,1024]{1,0:T(8,128)S(1)} %fusion.2, bf16[768,2048]{1,0:T(8,128)(2,1)S(1)} %reshape.85, bf16[1,2048,1024]{2,1,0:T(8,128)(2,1)S(1)} %copy-done.4), kind=kOutput, calls=%fused_computation.10 | convolution fusion | flops 3229089792 | bytes 12058624 | tf_op jit(solution)/shard_map/dot_general | solution.py:19
  88.2 0.0 copy-done.5
  88.2 3.6 %fusion.6 = bf16[768,2048]{1,0:T(8,128)(2,1)S(1)} fusion(bf16[768,1024]{1,0:T(8,128)(2,1)S(1)} %multiply_convert_fusion, bf16[1,1024,2048]{2,1,0:T(8,128)(2,1)S(1)} %copy-done.5), kind=kOutput, calls=%fused_computation.8 | convolution fusion | flops 3222798336 | bytes 8912896 | tf_op jit(solution)/shard_map/dot_general | solution.py:25
  91.9 2.9 %reshape.86 = bf16[128,6,2048]{2,1,0:T(8,128)(2,1)} reshape(bf16[768,2048]{1,0:T(8,128)(2,1)S(1)} %fusion.6) | data formatting | bytes 6291456 | tf_op jit(solution)/shard_map/reshape | solution.py:83
  94.7 0.0 copy-start
  94.7 0.0 copy-start.1
  94.7 5.2 %all-to-all-start.1 = ((bf16[128,6,2048]{2,1,0:T(8,128)(2,1)}), bf16[128,6,2048]{2,1,0:T(8,128)(2,1)}, u32[]{:S(2)}, u32[]{:S(2)}) async-start(bf16[128,6,2048]{2,1,0:T(8,128)(2,1)} %reshape.86), calls=%async_computation.1 | async-start | bytes 8388608 | tf_op jit(solution)/shard_map/all_to_all | solution.py:82
  99.9 0.0 copy-done
  99.9 0.0 copy-done.1
  99.9 0.0 copy-start.3
  99.9 0.0 copy-start.2
  99.9 0.4 multiply_convert_fusion.1
  100.3 0.0 copy-start.6
  100.4 3.6 %collective-permute-start = (bf16[2,1024]{1,0:T(2,128)(2,1)S(1)}, bf16[2,1024]{1,0:T(2,128)(2,1)S(1)}, u32[]{:S(2)}, u32[]{:S(2)}) collective-permute-start(bf16[2,1024]{1,0:T(2,128)(2,1)S(1)} %slice.38), channel_id=1, source_target_pairs={{0,1},{1,2},{2,3},{3,4},{4,5},{5,6},{6,7},{7,8},{8,9},{9,10},{10,1... | collective-permute-start | bytes 12296 | tf_op jit(solution)/shard_map/ppermute | solution.py:14
  104.0 0.1 mul.119
  104.1 0.0 copy-done.3
  104.1 0.0 copy-done.2
  104.2 0.1 copy.28
  104.3 42.4 %collective-permute-done = bf16[2,1024]{1,0:T(2,128)(2,1)S(1)} collective-permute-done((bf16[2,1024]{1,0:T(2,128)(2,1)S(1)}, bf16[2,1024]{1,0:T(2,128)(2,1)S(1)}, u32[]{:S(2)}, u32[]{:S(2)}) %collective-permute-start) | collective-permute-done | bytes 4128 | tf_op jit(solution)/shard_map/ppermute | solution.py:14
  146.7 0.3 maximum_convert_fusion
  147.0 0.0 copy-done.6
  147.0 6.1 %convolution_convert_fusion.1 = bf16[512,2048]{1,0:T(8,128)(2,1)} fusion(bf16[1024,2048]{1,0:T(8,128)(2,1)} %param.16, f32[514,1024]{1,0:T(8,128)S(1)} %maximum_convert_fusion, bf16[512,1024]{1,0:T(8,128)(2,1)S(1)} %copy-done.6, f32[1024]{0:T(1024)S(1)} %bitcast.42, f32[1024]{0:T(1024)S(1)} %bitcast.43, f32[1024]{0:T(1024)S(1)} %bitcast.41), kind=kOutput, calls=%fused_computation.11 | convolution fusion | flops 2152726528 | bytes 13643776 | tf_op jit(solution)/shard_map/dot_general | solution.py:51
  153.2 0.0 all-to-all-done.1
  153.2 4.9 %reshape.87 = bf16[768,2048]{1,0:T(8,128)(2,1)S(1)} reshape(bf16[128,6,2048]{2,1,0:T(8,128)(2,1)} %all-to-all-done.1) | data formatting | bytes 6291456 | tf_op jit(solution)/shard_map/reshape | solution.py:85
  158.1 3.3 %gather_fusion = bf16[512,2048]{1,0:T(8,128)(2,1)} fusion(bf16[768,2048]{1,0:T(8,128)(2,1)S(1)} %reshape.87, s32[1024]{0:T(1024)S(1)} %pad_clamp_fusion), kind=kCustom, calls=%fused_computation | custom fusion | bytes 4196352 | tf_op jit(solution)/shard_map/gather | solution.py:87
  161.4 4.8 %reshape.88 = f32[128,4,2048]{2,1,0:T(4,128)} reshape(bf16[512,2048]{1,0:T(8,128)(2,1)} %gather_fusion) | data formatting | bytes 6291456 | tf_op jit(solution)/shard_map/convert_element_type | solution.py:87
  166.2 6.2 %multiply_reduce_fusion = bf16[128,2048]{1,0:T(8,128)(2,1)} fusion(f32[128,4,2048]{2,1,0:T(4,128)} %reshape.88, f32[128,4]{1,0:T(8,128)S(1)} %copy.28), kind=kLoop, calls=%fused_computation.7 | loop fusion | flops 1835008 | bytes 4720640 | tf_op jit(solution)/shard_map/reduce_sum | solution.py:89
  (14 shorter events, 0.2 us)
Async XLA Ops:
  78.8 5.4 %copy-start.4 = (bf16[1,2048,1024]{2,1,0:T(8,128)(2,1)S(1)}, bf16[1,2048,1024]{2,1,0:T(8,128)(2,1)}, u32[]{:S(2)}) copy-start(bf16[1,2048,1024]{2,1,0:T(8,128)(2,1)} %param.22) | copy-start | bytes 12582916
  84.2 4.0 %copy-start.5 = (bf16[1,1024,2048]{2,1,0:T(8,128)(2,1)S(1)}, bf16[1,1024,2048]{2,1,0:T(8,128)(2,1)}, u32[]{:S(2)}) copy-start(bf16[1,1024,2048]{2,1,0:T(8,128)(2,1)} %param.23) | copy-start | bytes 12582916
  94.7 5.2 %copy-start = (bf16[512,1024]{1,0:T(8,128)(2,1)S(1)}, bf16[512,1024]{1,0:T(8,128)(2,1)}, u32[]{:S(2)}) copy-start(bf16[512,1024]{1,0:T(8,128)(2,1)} %param.14) | copy-start | bytes 3145732
  94.7 5.2 %copy-start.1 = (bf16[512,1024]{1,0:T(8,128)(2,1)S(1)}, bf16[512,1024]{1,0:T(8,128)(2,1)}, u32[]{:S(2)}) copy-start(bf16[512,1024]{1,0:T(8,128)(2,1)} %param.13) | copy-start | bytes 3145732
  94.7 58.5 %all-to-all-start.1 = ((bf16[128,6,2048]{2,1,0:T(8,128)(2,1)}), bf16[128,6,2048]{2,1,0:T(8,128)(2,1)}, u32[]{:S(2)}, u32[]{:S(2)}) async-start(bf16[128,6,2048]{2,1,0:T(8,128)(2,1)} %reshape.86), calls=%async_computation.1 | async-start | bytes 8388608 | tf_op jit(solution)/shard_map/all_to_all | solution.py:82
  99.9 4.2 %copy-start.3 = (f32[128,4]{0,1:T(4,128)S(1)}, f32[128,4]{0,1:T(4,128)}, u32[]{:S(2)}) copy-start(f32[128,4]{0,1:T(4,128)} %param.20) | copy-start | bytes 6148
  99.9 4.2 %copy-start.2 = (f32[3,1024]{1,0:T(4,128)S(1)}, f32[3,1024]{1,0:T(4,128)}, u32[]{:S(2)}) copy-start(f32[3,1024]{1,0:T(4,128)} %param.15) | copy-start | bytes 36868
  100.3 46.7 %copy-start.6 = (bf16[512,1024]{1,0:T(8,128)(2,1)S(1)}, bf16[512,1024]{1,0:T(8,128)(2,1)}, u32[]{:S(2)}) copy-start(bf16[512,1024]{1,0:T(8,128)(2,1)} %param.12) | copy-start | bytes 3145732
  100.4 46.4 %collective-permute-start = (bf16[2,1024]{1,0:T(2,128)(2,1)S(1)}, bf16[2,1024]{1,0:T(2,128)(2,1)S(1)}, u32[]{:S(2)}, u32[]{:S(2)}) collective-permute-start(bf16[2,1024]{1,0:T(2,128)(2,1)S(1)} %slice.38), channel_id=1, source_target_pairs={{0,1},{1,2},{2,3},{3,4},{4,5},{5,6},{6,7},{7,8},{8,9},{9,10},{10,1... | collective-permute-start | bytes 12296 | tf_op jit(solution)/shard_map/ppermute | solution.py:14
where the time goes:
time: 173 us; the launch traced here: 172 us
  blocking collectives  65 us (38%)
  waiting for transfers between devices  42.4 us (25%)
  local copies, waits for them, and re-layouts  25.1 us (15%)
  matrix products  21.2 us (12%)
  other arithmetic  8.92 us (5%)
  starting transfers between devices  8.75 us (5%)
    all_to_all x1, blocking collectives, shards(): lax.all_to_all(send_rows, ('ep', 'tp'), split_axis=0, concat_axis=0, tile...  65 us
    ppermute x1, waiting for transfers between devices, from_behind(): return lax.ppermute(value, axis, pairs)  42.4 us
    reduce_sum x1, other arithmetic, shards(): jnp.sum(picked * mix_weight[:, :, None], axis=1).astype(jnp.bfloat16)  6.2 us
    dot_general x1, matrix products, shards(): jnp.dot(gated_rows, mixer_out_weight, preferred_element_type=jnp.float32)  6.14 us
    dot_general x1, matrix products, expert_rows(): jnp.dot(row_block, gate_weight, preferred_element_type=jnp.float32)  5.35 us
    all_to_all x1, starting transfers between devices, shards(): lax.all_to_all(expert_out.reshape(received.shape), ('ep', 'tp'), split_ax...  5.16 us
    reshape x1, local copies, waits for them, and re-layouts, shards(): flat_rows = returned.reshape(experts_all * capacity, width)  4.87 us
    reshape x1, local copies, waits for them, and re-layouts, shards(): row_block = received.reshape(-1, width)  4.87 us
  transfers between devices with their start and end apart: 2, of which 1 were waited for; matrix products, arithmetic and copies ran while one was open for 4% of the time, Pallas kernels for 0%

commit v1 on v0

v1 whole, which is shorter than its diff:
```python
import functools

import jax
import jax.numpy as jnp
import numpy as np
from jax import lax
from jax.experimental import pallas as pl
from jax.experimental.pallas import tpu as pltpu
from jax.sharding import PartitionSpec as P

epsilon = 1e-06
clamp_limit = 7.0
alpha_gate = 1.702
MESH = pl.DeviceIdType.MESH

SIDE = 4
CORES = 2


def peer_order():
    def hops(off):
        return sum(min(v, SIDE - v) for v in off[:3])

    offs = [
        (dz, dy, dx, dk)
        for dz in range(SIDE)
        for dy in range(SIDE)
        for dx in range(SIDE)
        for dk in range(CORES)
    ][1:]
    state = 12345
    keyed = []
    for off in offs:
        state = (state * 1103515245 + 12345) % (1 << 31)
        keyed.append((-hops(off), state >> 8, off))
    return [k[2] for k in sorted(keyed)] + [(0, 0, 0, 0)]


ORDER = peer_order()
PEERS = len(ORDER)
GROUP = 8
CHUNK = 16
CHUNKS = PEERS // CHUNK
ROWS = CHUNK * GROUP


def kernel(
    cap,
    go_hbm,
    gi_hbm,
    ci_hbm,
    taps_hbm,
    wmix_hbm,
    tok_hbm,
    gain_hbm,
    ids_hbm,
    rw_hbm,
    offs_hbm,
    wg_hbm,
    wu_hbm,
    wd_hbm,
    mixed_hbm,
    moe_hbm,
    go,
    gi,
    ci,
    taps,
    wmix,
    tok,
    gain,
    ids,
    rw,
    offs,
    wg,
    wu,
    wd,
    mixed,
    moe,
    send,
    recv,
    ret,
    pick,
    comb,
    prod,
    tail,
    halo,
    normed,
    acc,
    lsem,
    osem,
    dsend,
    drecv,
    rsend,
    rrecv,
    hsem,
):
    ep = lax.axis_index("ep")
    tp = lax.axis_index("tp")
    z = ep // (SIDE * CORES)
    y = (ep // CORES) % SIDE
    k = ep % CORES
    x = tp

    def local(i, src, dst):
        copy = pltpu.make_async_copy(src, dst, lsem.at[i])
        copy.start()
        return copy

    small = [
        local(0, tok_hbm, tok),
        local(1, ids_hbm, ids),
        local(2, rw_hbm, rw),
        local(3, gain_hbm, gain),
        local(4, offs_hbm, offs),
    ]

    zs = [(z + d) % SIDE * (SIDE * CORES) for d in range(SIDE)]
    zn = [(z + SIDE - d) % SIDE * (SIDE * CORES) for d in range(SIDE)]
    ys = [(y + d) % SIDE * CORES for d in range(SIDE)]
    yn = [(y + SIDE - d) % SIDE * CORES for d in range(SIDE)]
    xs = [(x + d) % SIDE for d in range(SIDE)]
    xn = [(x + SIDE - d) % SIDE for d in range(SIDE)]
    ks = [(k + d) % CORES for d in range(CORES)]

    def ahead(i):
        dz, dy, dx, dk = ORDER[i]
        return (zs[dz] + ys[dy] + ks[dk], xs[dx])

    def behind(i):
        dz, dy, dx, dk = ORDER[i]
        return (zn[dz] + yn[dy] + ks[dk], xn[dx])

    barrier = pltpu.get_barrier_semaphore()
    for i in range(PEERS - 1):
        pl.semaphore_signal(barrier, inc=1, device_id=ahead(i), device_id_type=MESH)

    mix_in = [
        local(5, gi_hbm, gi),
        local(6, ci_hbm, ci),
        local(7, go_hbm, go),
        local(8, taps_hbm, taps),
        local(9, wmix_hbm, wmix),
    ]
    experts_in = [
        local(10, wg_hbm, wg),
        local(11, wu_hbm, wu),
        local(12, wd_hbm, wd),
    ]

    for copy in small:
        copy.wait()
    wide = tok[...].astype(jnp.float32)
    mean = jnp.mean(wide * wide, axis=-1, keepdims=True)
    normed[...] = (wide * lax.rsqrt(mean + epsilon) * gain[...]).astype(jnp.bfloat16)

    tokens = tok.shape[0]
    off = offs[...]
    oz, oy, ok, ox = off // 32, (off // 8) % SIDE, (off // 4) % CORES, off % SIDE
    target = (
        (z + oz) % SIDE * 32 + (y + oy) % SIDE * 8 + (k + ok) % CORES * 4 + (x + ox) % SIDE
    )
    weights = rw[...]
    weights = weights / jnp.sum(weights, axis=0, keepdims=True)
    named = jnp.zeros((PEERS, tokens), jnp.float32)
    named_weight = jnp.zeros((PEERS, tokens), jnp.float32)
    for j in range(ids.shape[0]):
        hit = ids[j : j + 1, :] == target
        named = jnp.where(hit, 1.0, named)
        named_weight = jnp.where(hit, weights[j : j + 1, :], named_weight)
    earlier = (
        lax.broadcasted_iota(jnp.int32, (tokens, tokens), 0)
        < lax.broadcasted_iota(jnp.int32, (tokens, tokens), 1)
    ).astype(jnp.bfloat16)
    rank = jnp.dot(named.astype(jnp.bfloat16), earlier, preferred_element_type=jnp.float32)
    rank = jnp.where(named > 0.5, rank, 99.0)
    place = lax.broadcasted_iota(jnp.int32, (PEERS, GROUP, tokens), 1).astype(jnp.float32)
    chosen = jnp.broadcast_to(rank[:, None, :], (PEERS, GROUP, tokens)) == place
    pick[...] = (
        jnp.where(chosen, 1.0, 0.0).reshape(PEERS * GROUP, tokens).astype(jnp.bfloat16)
    )

    def dispatch(i):
        rows = pl.ds(i * GROUP, cap)
        return pltpu.make_async_remote_copy(
            send.at[rows],
            recv.at[rows],
            dsend,
            drecv.at[i // CHUNK],
            device_id=ahead(i),
            device_id_type=MESH,
        )

    def giveback(i):
        rows = pl.ds(i * GROUP, cap)
        return pltpu.make_async_remote_copy(
            recv.at[rows],
            ret.at[rows],
            rsend,
            rrecv.at[i // CHUNK],
            device_id=behind(i),
            device_id_type=MESH,
        )

    def peers_of(c):
        return range(c * CHUNK, min((c + 1) * CHUNK, PEERS - 1))

    def all_rows(ref, sem, count):
        part = ref.at[pl.ds(0, count * GROUP), pl.ds(0, ref.shape[1] * cap // GROUP)]
        return pltpu.make_async_copy(part, part, sem)

    for c in range(CHUNKS):
        rows = pl.ds(c * ROWS, ROWS)
        send[rows, :] = jnp.dot(
            pick[rows, :], normed[...], preferred_element_type=jnp.float32
        ).astype(jnp.bfloat16)
        if c == 0:
            pl.semaphore_wait(barrier, PEERS - 1)
        else:
            for i in peers_of(c - 1):
                dispatch(i).start()
    for i in peers_of(CHUNKS - 1):
        dispatch(i).start()
    own = pl.ds((PEERS - 1) * GROUP, GROUP)
    recv[own, :] = send[own, :]

    reach = taps.shape[0] - 1
    positions = gi.shape[0]
    for copy in mix_in[:2]:
        copy.wait()
    last = pl.ds(positions - 16, 16)
    tail[...] = (gi[last, :].astype(jnp.float32) * ci[last, :].astype(jnp.float32)).astype(
        jnp.bfloat16
    )
    here = ep * SIDE + tp
    after = (here + 1) % PEERS
    halo_copy = pltpu.make_async_remote_copy(
        tail.at[pl.ds(8, 8)],
        halo.at[pl.ds(8, 8)],
        hsem.at[0],
        hsem.at[1],
        device_id=(after // SIDE, after % SIDE),
        device_id_type=MESH,
    )
    halo_copy.start()

    block = 128

    @pl.loop(0, positions // block)
    def _(b):
        rows = pl.ds(pl.multiple_of(b * block, block), block)
        prod[pl.ds(pl.multiple_of(8 + b * block, 8), block), :] = (
            (gi[rows, :].astype(jnp.float32) * ci[rows, :].astype(jnp.float32))
            .astype(jnp.bfloat16)
            .astype(jnp.float32)
        )

    for c in range(CHUNKS):
        group = rank[c * CHUNK : (c + 1) * CHUNK]
        group_weight = named_weight[c * CHUNK : (c + 1) * CHUNK]
        shape = (CHUNK, GROUP, tokens)
        share = jnp.where(
            jnp.broadcast_to(group[:, None, :], shape) == place[:CHUNK],
            jnp.broadcast_to(group_weight[:, None, :], shape),
            0.0,
        ).reshape(ROWS, tokens)
        comb[c] = share.T.astype(jnp.bfloat16)

    for copy in mix_in[2:]:
        copy.wait()
    halo_copy.wait()
    prod[0:8, :] = jnp.where(here == 0, 0.0, halo[8:16, :].astype(jnp.float32))

    @pl.loop(0, positions // block)
    def _(b):
        rows = pl.ds(pl.multiple_of(b * block, block), block)
        window = prod[pl.ds(pl.multiple_of(b * block, 8), block + 8), :]
        convolved = jnp.zeros((block, window.shape[1]), jnp.float32)
        for j in range(reach + 1):
            start = 8 - reach + j
            convolved = convolved + taps[j : j + 1, :] * window[start : start + block]
        gated = (go[rows, :].astype(jnp.float32) * convolved).astype(jnp.bfloat16)
        mixed[rows, :] = jnp.dot(
            gated, wmix[...], preferred_element_type=jnp.float32
        ).astype(jnp.bfloat16)

    mixed_copy = pltpu.make_async_copy(mixed, mixed_hbm, osem.at[0])
    mixed_copy.start()

    for copy in experts_in:
        copy.wait()

    @pl.loop(0, CHUNKS)
    def _(c):
        for n in range(CHUNKS):

            @pl.when(c == n)
            def _():
                all_rows(recv, drecv.at[n], len(peers_of(n))).wait()

        rows = pl.ds(pl.multiple_of(c * ROWS, ROWS), ROWS)
        block_rows = recv[rows, :]
        hidden = []
        width = 256
        for n in range(0, wg.shape[1], width):
            gate_pre = jnp.dot(
                block_rows, wg[:, n : n + width], preferred_element_type=jnp.float32
            )
            up_pre = jnp.dot(
                block_rows, wu[:, n : n + width], preferred_element_type=jnp.float32
            )
            gate_pre = jnp.minimum(gate_pre, clamp_limit)
            up_pre = jnp.clip(up_pre, -clamp_limit, clamp_limit)
            hidden.append(
                ((up_pre + 1.0) * (gate_pre * jax.nn.sigmoid(alpha_gate * gate_pre))).astype(
                    jnp.bfloat16
                )
            )
        hidden = jnp.concatenate(hidden, axis=1)
        for n in range(0, wd.shape[1], width):
            recv[rows, n : n + width] = jnp.dot(
                hidden, wd[:, n : n + width], preferred_element_type=jnp.float32
            ).astype(jnp.bfloat16)
        for n in range(CHUNKS):

            @pl.when(c == n)
            def _():
                for i in peers_of(n):
                    giveback(i).start()

    ret[own, :] = recv[own, :]

    acc[...] = jnp.zeros_like(acc)
    used = lax.broadcasted_iota(jnp.int32, (ROWS, ret.shape[1]), 0) % GROUP < cap

    @pl.loop(0, CHUNKS)
    def _(c):
        for n in range(CHUNKS):

            @pl.when(c == n)
            def _():
                all_rows(ret, rrecv.at[n], len(peers_of(n))).wait()

        rows = pl.ds(pl.multiple_of(c * ROWS, ROWS), ROWS)
        back = jnp.where(used, ret[rows, :].astype(jnp.float32), 0.0).astype(jnp.bfloat16)
        acc[...] += jnp.dot(comb[c], back, preferred_element_type=jnp.float32)

    moe[...] = acc[...].astype(jnp.bfloat16)
    moe_copy = pltpu.make_async_copy(moe, moe_hbm, osem.at[1])
    moe_copy.start()
    all_rows(send, dsend, PEERS - 1).wait()
    all_rows(recv, rsend, PEERS - 1).wait()
    mixed_copy.wait()
    moe_copy.wait()


def shards(
    gate_outer,
    gate_inner,
    conv_input,
    conv_taps,
    mixer_out_weight,
    moe_tokens,
    norm_gain,
    expert_ids,
    route_weight,
    expert_gate,
    expert_up,
    expert_down,
):
    positions, channels = gate_inner.shape
    tokens, width = moe_tokens.shape
    hidden = expert_gate.shape[2]
    choices = expert_ids.shape[1]
    cap = 3 * tokens * choices // (2 * PEERS)
    offsets = np.array([dz * 32 + dy * 8 + dk * 4 + dx for dz, dy, dx, dk in ORDER], np.int32)
    offsets = jnp.asarray(np.broadcast_to(offsets[:, None], (PEERS, tokens)))
    bf16, f32 = jnp.bfloat16, jnp.float32
    anywhere = pl.BlockSpec(memory_space=pl.ANY)
    slots = (PEERS * GROUP, width)
    return pl.pallas_call(
        functools.partial(kernel, cap),
        out_shape=(
            jax.ShapeDtypeStruct((positions, width), bf16),
            jax.ShapeDtypeStruct((tokens, width), bf16),
        ),
        in_specs=[anywhere] * 13,
        out_specs=(anywhere, anywhere),
        scratch_shapes=[
            pltpu.VMEM((positions, channels), bf16),
            pltpu.VMEM((positions, channels), bf16),
            pltpu.VMEM((positions, channels), bf16),
            pltpu.VMEM(conv_taps.shape, f32),
            pltpu.VMEM((channels, width), bf16),
            pltpu.VMEM((tokens, width), bf16),
            pltpu.VMEM((1, width), f32),
            pltpu.VMEM((choices, tokens), jnp.int32),
            pltpu.VMEM((choices, tokens), f32),
            pltpu.VMEM((PEERS, tokens), jnp.int32),
            pltpu.VMEM((width, hidden), bf16),
            pltpu.VMEM((width, hidden), bf16),
            pltpu.VMEM((hidden, width), bf16),
            pltpu.VMEM((positions, width), bf16),
            pltpu.VMEM((tokens, width), bf16),
            pltpu.VMEM(slots, bf16),
            pltpu.VMEM(slots, bf16),
            pltpu.VMEM(slots, bf16),
            pltpu.VMEM((PEERS * GROUP, tokens), bf16),
            pltpu.VMEM((CHUNKS, tokens, ROWS), bf16),
            pltpu.VMEM((8 + positions, channels), f32),
            pltpu.VMEM((16, channels), bf16),
            pltpu.VMEM((16, channels), bf16),
            pltpu.VMEM((tokens, width), bf16),
            pltpu.VMEM((tokens, width), f32),
            pltpu.SemaphoreType.DMA((13,)),
            pltpu.SemaphoreType.DMA((2,)),
            pltpu.SemaphoreType.DMA,
            pltpu.SemaphoreType.DMA((CHUNKS,)),
            pltpu.SemaphoreType.DMA,
            pltpu.SemaphoreType.DMA((CHUNKS,)),
            pltpu.SemaphoreType.DMA((2,)),
        ],
        compiler_params=pltpu.CompilerParams(
            collective_id=0, has_side_effects=True, vmem_limit_bytes=62 * 2**20
        ),
        name="layer_step",
    )(
        gate_outer,
        gate_inner,
        conv_input,
        conv_taps,
        mixer_out_weight,
        moe_tokens,
        norm_gain.reshape(1, width),
        expert_ids.T,
        route_weight.T,
        offsets,
        expert_gate.reshape(width, hidden),
        expert_up.reshape(width, hidden),
        expert_down.reshape(hidden, width),
    )


def solution(mesh):
    rows = P(("ep", "tp"), None)
    experts = P(("ep", "tp"), None, None)
    in_specs = (rows, rows, rows, P(), P(), rows, P(), rows, rows, experts, experts, experts)
    return jax.shard_map(
        shards, mesh=mesh, in_specs=in_specs, out_specs=(rows, rows), check_vma=False
    )
```

time: 173 us -> 98.4 us (0.57)
  Pallas kernels: 0 us -> 91.5 us
  blocking collectives: 65 us -> 0 us
  waiting for transfers between devices: 42.4 us -> 0 us
  matrix products: 21.2 us -> 0 us
  local copies, waits for them, and re-layouts: 25.1 us -> 5.38 us
  other arithmetic: 8.92 us -> 0 us
  starting transfers between devices: 8.75 us -> 0 us
    pallas_call x0 -> x1, Pallas kernels: none -> 91.5 us  [shards(): pl.pallas_call(functools.partial(kernel, cap), out_shape=(jax.ShapeDtypeS...]
    all_to_all x1 -> x0, blocking collectives: 65 us -> none  [shards(): lax.all_to_all(send_rows, ('ep', 'tp'), split_axis=0, concat_axis=0, tile...]
    ppermute x1 -> x0, waiting for transfers between devices: 42.4 us -> none  [from_behind(): return lax.ppermute(value, axis, pairs)]
    dot_general x5 -> x0, matrix products: 21.2 us -> none  [the longest x1 6.14 us: shards(): jnp.dot(gated_rows, mixer_out_weight, preferred_element_type=jnp.float32)]
    reshape x4 -> x0, local copies, waits for them, and re-layouts: 15.5 us -> none  [the longest x1 4.87 us: shards(): flat_rows = returned.reshape(experts_all * capacity, width)]
    reduce_sum x4 -> x0, other arithmetic: 7.68 us -> none  [the longest x1 6.2 us: shards(): jnp.sum(picked * mix_weight[:, :, None], axis=1).astype(jnp.bfloat16)]
    all_to_all x1 -> x0, starting transfers between devices: 5.16 us -> none  [shards(): lax.all_to_all(expert_out.reshape(received.shape), ('ep', 'tp'), split_ax...]
    convert_element_type x1 -> x0, local copies, waits for them, and re-layouts: 4.75 us -> none  [shards(): flat_rows[slot_index.reshape(-1)].astype(jnp.float32)]
  transfers between devices with their start and end apart: 2 -> 0, of which waited for: 1 -> 0; matrix products, arithmetic and copies ran while one was open for 4% -> 0% of each run, Pallas kernels for 0% -> 0%
where the time goes in v1:
time: 98.4 us; the launch traced here: 97.5 us
  Pallas kernels  91.5 us (93%)
  local copies, waits for them, and re-layouts  5.38 us (5%)
    pallas_call x1, Pallas kernels, shards(): pl.pallas_call(functools.partial(kernel, cap), out_shape=(jax.ShapeDtypeS...  91.5 us
    unnamed x4, local copies, waits for them, and re-layouts  4.01 us

profile of v1, /device:TPU:1, one launch (start us, length us, event | category | flops | bytes accessed | tf_op | source)
XLA Modules:
  0.0 97.5 jit_solution(11759287743645174843)
XLA Ops:
  0.6 1.4 %jit_solution_.3.offs_hbm = s32[128,128]{1,0:T(8,128)} broadcast(s32[128]{0:T(128)} %constant.2.clone), dimensions={0} | broadcast | bytes 66048 | tf_op jit(solution)
  2.0 91.5 %layer_step.1 = (bf16[512,2048]{1,0:T(8,128)(2,1)}, bf16[128,2048]{1,0:T(8,128)(2,1)}) custom-call(bf16[512,1024]{1,0:T(8,128)(2,1)} %go_hbm.1, bf16[512,1024]{1,0:T(8,128)(2,1)} %gi_hbm.1, bf16[512,1024]{1,0:T(8,128)(2,1)} %ci_hbm.1, f32[3,1024]{1,0:T(4,128)} %taps_hbm.1, bf16[1024,2048]{1,0:T(8,128)(2,1)} %wmix_hbm.1, bf16[128,2048]{1,0:T(8,128)(2,1)} %tok_hbm.1, ...), custom_call_target="tpu_custom_call" | custom-call | tf_op jit(solution)/shard_map/layer_step/pallas_call | solution.py:380
  93.5 0.0 copy-start
  93.5 3.2 %copy.17 = bf16[512,2048]{1,0:T(8,128)(2,1)} copy(bf16[512,2048]{1,0:T(8,128)(2,1)} %get-tuple-element.4) | data formatting | bytes 4194304
  96.7 0.0 copy-done
  96.7 0.8 copy.18
Async XLA Ops:
  93.5 3.2 %copy-start = (bf16[128,2048]{1,0:T(8,128)(2,1)S(1)}, bf16[128,2048]{1,0:T(8,128)(2,1)}, u32[]{:S(2)}) copy-start(bf16[128,2048]{1,0:T(8,128)(2,1)} %get-tuple-element.5) | copy-start | bytes 1572868

commit v2 on v1

--- a/solution.py
+++ b/solution.py
@@ -2,7 +2,6 @@
 
 import jax
 import jax.numpy as jnp
-import numpy as np
 from jax import lax
 from jax.experimental import pallas as pl
 from jax.experimental.pallas import tpu as pltpu
@@ -55,12 +54,11 @@
     gain_hbm,
     ids_hbm,
     rw_hbm,
-    offs_hbm,
     wg_hbm,
     wu_hbm,
     wd_hbm,
-    mixed_hbm,
-    moe_hbm,
+    mixed,
+    moe,
     go,
     gi,
     ci,
@@ -70,24 +68,21 @@
     gain,
     ids,
     rw,
-    offs,
     wg,
     wu,
     wd,
-    mixed,
-    moe,
     send,
     recv,
     ret,
     pick,
     comb,
     prod,
+    tails,
     tail,
     halo,
     normed,
     acc,
     lsem,
-    osem,
     dsend,
     drecv,
     rsend,
@@ -106,12 +101,15 @@
         copy.start()
         return copy
 
+    positions = gi.shape[0]
+    last = pl.ds(positions - 16, 16)
     small = [
         local(0, tok_hbm, tok),
         local(1, ids_hbm, ids),
         local(2, rw_hbm, rw),
         local(3, gain_hbm, gain),
-        local(4, offs_hbm, offs),
+        local(4, gi_hbm.at[last], tails.at[0]),
+        local(13, ci_hbm.at[last], tails.at[1]),
     ]
 
     zs = [(z + d) % SIDE * (SIDE * CORES) for d in range(SIDE)]
@@ -153,8 +151,28 @@
     mean = jnp.mean(wide * wide, axis=-1, keepdims=True)
     normed[...] = (wide * lax.rsqrt(mean + epsilon) * gain[...]).astype(jnp.bfloat16)
 
+    tail[...] = (tails[0].astype(jnp.float32) * tails[1].astype(jnp.float32)).astype(jnp.bfloat16)
+    here = ep * SIDE + tp
+    after = (here + 1) % PEERS
+    halo_copy = pltpu.make_async_remote_copy(
+        tail.at[pl.ds(8, 8)],
+        halo.at[pl.ds(8, 8)],
+        hsem.at[0],
+        hsem.at[1],
+        device_id=(after // SIDE, after % SIDE),
+        device_id_type=MESH,
+    )
+
     tokens = tok.shape[0]
-    off = offs[...]
+    sublane = lax.broadcasted_iota(jnp.int32, (GROUP, tokens), 0)
+    off = []
+    for i in range(0, PEERS, GROUP):
+        codes = [dz * 32 + dy * 8 + dk * 4 + dx for dz, dy, dx, dk in ORDER[i : i + GROUP]]
+        part = jnp.full((GROUP, tokens), codes[0], jnp.int32)
+        for j in range(1, GROUP):
+            part = jnp.where(sublane == j, codes[j], part)
+        off.append(part)
+    off = jnp.concatenate(off, axis=0)
     oz, oy, ok, ox = off // 32, (off // 8) % SIDE, (off // 4) % CORES, off % SIDE
     target = (
         (z + oz) % SIDE * 32 + (y + oy) % SIDE * 8 + (k + ok) % CORES * 4 + (x + ox) % SIDE
@@ -214,7 +232,9 @@
             pick[rows, :], normed[...], preferred_element_type=jnp.float32
         ).astype(jnp.bfloat16)
         if c == 0:
-            pl.semaphore_wait(barrier, PEERS - 1)
+            with jax.named_scope("barrier"):
+                pl.semaphore_wait(barrier, PEERS - 1)
+            halo_copy.start()
         else:
             for i in peers_of(c - 1):
                 dispatch(i).start()
@@ -224,25 +244,8 @@
     recv[own, :] = send[own, :]
 
     reach = taps.shape[0] - 1
-    positions = gi.shape[0]
     for copy in mix_in[:2]:
         copy.wait()
-    last = pl.ds(positions - 16, 16)
-    tail[...] = (gi[last, :].astype(jnp.float32) * ci[last, :].astype(jnp.float32)).astype(
-        jnp.bfloat16
-    )
-    here = ep * SIDE + tp
-    after = (here + 1) % PEERS
-    halo_copy = pltpu.make_async_remote_copy(
-        tail.at[pl.ds(8, 8)],
-        halo.at[pl.ds(8, 8)],
-        hsem.at[0],
-        hsem.at[1],
-        device_id=(after // SIDE, after % SIDE),
-        device_id_type=MESH,
-    )
-    halo_copy.start()
-
     block = 128
 
     @pl.loop(0, positions // block)
@@ -267,7 +270,8 @@
 
     for copy in mix_in[2:]:
         copy.wait()
-    halo_copy.wait()
+    with jax.named_scope('halo_wait'):
+        halo_copy.wait()
     prod[0:8, :] = jnp.where(here == 0, 0.0, halo[8:16, :].astype(jnp.float32))
 
     @pl.loop(0, positions // block)
@@ -283,11 +287,9 @@
             gated, wmix[...], preferred_element_type=jnp.float32
         ).astype(jnp.bfloat16)
 
-    mixed_copy = pltpu.make_async_copy(mixed, mixed_hbm, osem.at[0])
-    mixed_copy.start()
-
-    for copy in experts_in:
-        copy.wait()
+    with jax.named_scope('expw_wait'):
+        for copy in experts_in:
+            copy.wait()
 
     @pl.loop(0, CHUNKS)
     def _(c):
@@ -295,7 +297,8 @@
 
             @pl.when(c == n)
             def _():
-                all_rows(recv, drecv.at[n], len(peers_of(n))).wait()
+                with jax.named_scope('dwait'):
+                    all_rows(recv, drecv.at[n], len(peers_of(n))).wait()
 
         rows = pl.ds(pl.multiple_of(c * ROWS, ROWS), ROWS)
         block_rows = recv[rows, :]
@@ -338,19 +341,17 @@
 
             @pl.when(c == n)
             def _():
-                all_rows(ret, rrecv.at[n], len(peers_of(n))).wait()
+                with jax.named_scope('rwait'):
+                    all_rows(ret, rrecv.at[n], len(peers_of(n))).wait()
 
         rows = pl.ds(pl.multiple_of(c * ROWS, ROWS), ROWS)
         back = jnp.where(used, ret[rows, :].astype(jnp.float32), 0.0).astype(jnp.bfloat16)
         acc[...] += jnp.dot(comb[c], back, preferred_element_type=jnp.float32)
 
     moe[...] = acc[...].astype(jnp.bfloat16)
-    moe_copy = pltpu.make_async_copy(moe, moe_hbm, osem.at[1])
-    moe_copy.start()
-    all_rows(send, dsend, PEERS - 1).wait()
-    all_rows(recv, rsend, PEERS - 1).wait()
-    mixed_copy.wait()
-    moe_copy.wait()
+    with jax.named_scope('endwait'):
+        all_rows(send, dsend, PEERS - 1).wait()
+        all_rows(recv, rsend, PEERS - 1).wait()
 
 
 def shards(
@@ -372,19 +373,17 @@
     hidden = expert_gate.shape[2]
     choices = expert_ids.shape[1]
     cap = 3 * tokens * choices // (2 * PEERS)
-    offsets = np.array([dz * 32 + dy * 8 + dk * 4 + dx for dz, dy, dx, dk in ORDER], np.int32)
-    offsets = jnp.asarray(np.broadcast_to(offsets[:, None], (PEERS, tokens)))
     bf16, f32 = jnp.bfloat16, jnp.float32
     anywhere = pl.BlockSpec(memory_space=pl.ANY)
     slots = (PEERS * GROUP, width)
     return pl.pallas_call(
         functools.partial(kernel, cap),
         out_shape=(
-            jax.ShapeDtypeStruct((positions, width), bf16),
-            jax.ShapeDtypeStruct((tokens, width), bf16),
+            pltpu.VMEM((positions, width), bf16),
+            pltpu.VMEM((tokens, width), bf16),
         ),
-        in_specs=[anywhere] * 13,
-        out_specs=(anywhere, anywhere),
+        in_specs=[anywhere] * 12,
+        out_specs=(pl.BlockSpec(memory_space=pltpu.VMEM), pl.BlockSpec(memory_space=pltpu.VMEM)),
         scratch_shapes=[
             pltpu.VMEM((positions, channels), bf16),
             pltpu.VMEM((positions, channels), bf16),
@@ -395,24 +394,21 @@
             pltpu.VMEM((1, width), f32),
             pltpu.VMEM((choices, tokens), jnp.int32),
             pltpu.VMEM((choices, tokens), f32),
-            pltpu.VMEM((PEERS, tokens), jnp.int32),
             pltpu.VMEM((width, hidden), bf16),
             pltpu.VMEM((width, hidden), bf16),
             pltpu.VMEM((hidden, width), bf16),
-            pltpu.VMEM((positions, width), bf16),
-            pltpu.VMEM((tokens, width), bf16),
             pltpu.VMEM(slots, bf16),
             pltpu.VMEM(slots, bf16),
             pltpu.VMEM(slots, bf16),
             pltpu.VMEM((PEERS * GROUP, tokens), bf16),
             pltpu.VMEM((CHUNKS, tokens, ROWS), bf16),
             pltpu.VMEM((8 + positions, channels), f32),
+            pltpu.VMEM((2, 16, channels), bf16),
             pltpu.VMEM((16, channels), bf16),
             pltpu.VMEM((16, channels), bf16),
             pltpu.VMEM((tokens, width), bf16),
             pltpu.VMEM((tokens, width), f32),
-            pltpu.SemaphoreType.DMA((13,)),
-            pltpu.SemaphoreType.DMA((2,)),
+            pltpu.SemaphoreType.DMA((14,)),
             pltpu.SemaphoreType.DMA,
             pltpu.SemaphoreType.DMA((CHUNKS,)),
             pltpu.SemaphoreType.DMA,
@@ -420,7 +416,7 @@
             pltpu.SemaphoreType.DMA((2,)),
         ],
         compiler_params=pltpu.CompilerParams(
-            collective_id=0, has_side_effects=True, vmem_limit_bytes=62 * 2**20
+            collective_id=0, has_side_effects=True, vmem_limit_bytes=56 * 2**20
         ),
         name="layer_step",
     )(
@@ -433,7 +429,6 @@
         norm_gain.reshape(1, width),
         expert_ids.T,
         route_weight.T,
-        offsets,
         expert_gate.reshape(width, hidden),
         expert_up.reshape(width, hidden),
         expert_down.reshape(hidden, width),

time: 98.4 us -> 86 us (0.87)
  Pallas kernels: 91.5 us -> 82.9 us
  local copies, waits for them, and re-layouts: 5.38 us -> 2.11 us
    pallas_call x1, Pallas kernels: 91.5 us -> 82.9 us  [shards(): pl.pallas_call(functools.partial(kernel, cap), out_shape=(pltpu.VMEM((pos...]
    unnamed x4 -> x2, local copies, waits for them, and re-layouts: 4.01 us -> 2.11 us
    another operation x1 -> x0, local copies, waits for them, and re-layouts: 1.37 us -> none
where the time goes in v2:
time: 86 us; the launch traced here: 85.7 us
  Pallas kernels  82.9 us (96%)
  local copies, waits for them, and re-layouts  2.11 us (2%)
    pallas_call x1, Pallas kernels, shards(): pl.pallas_call(functools.partial(kernel, cap), out_shape=(pltpu.VMEM((pos...  82.9 us
    unnamed x2, local copies, waits for them, and re-layouts  2.11 us

profile of v2, /device:TPU:1, one launch (start us, length us, event | category | flops | bytes accessed | tf_op | source)
XLA Modules:
  0.0 85.7 jit_solution(16062897206280629112)
XLA Ops:
  0.6 82.9 %layer_step.1 = (bf16[512,2048]{1,0:T(8,128)(2,1)S(1)}, bf16[128,2048]{1,0:T(8,128)(2,1)S(1)}) custom-call(bf16[512,1024]{1,0:T(8,128)(2,1)} %go_hbm.1, bf16[512,1024]{1,0:T(8,128)(2,1)} %gi_hbm.1, bf16[512,1024]{1,0:T(8,128)(2,1)} %ci_hbm.1, f32[3,1024]{1,0:T(4,128)} %taps_hbm.1, bf16[1024,2048]{1,0:T(8,128)(2,1)} %wmix_hbm.1, bf16[128,2048]{1,0:T(8,128)(2,1)} %tok_hbm.1, ...), custom_call_target="tpu_custom_call" | custom-call | tf_op jit(solution)/shard_map/layer_step/pallas_call | solution.py:379
  83.6 1.3 %copy.16 = bf16[512,2048]{1,0:T(8,128)(2,1)} copy(bf16[512,2048]{1,0:T(8,128)(2,1)S(1)} %get-tuple-element.2) | data formatting | bytes 4194304
  84.9 0.8 copy.17

commit v3 on v2

--- a/solution.py
+++ b/solution.py
@@ -14,33 +14,40 @@
 
 SIDE = 4
 CORES = 2
-
-
-def peer_order():
-    def hops(off):
-        return sum(min(v, SIDE - v) for v in off[:3])
-
-    offs = [
-        (dz, dy, dx, dk)
-        for dz in range(SIDE)
-        for dy in range(SIDE)
-        for dx in range(SIDE)
-        for dk in range(CORES)
-    ][1:]
+AXES = 3
+
+
+def hops(off):
+    return sum(min(v, SIDE - v) for v in off[:AXES])
+
+
+def shuffled(offs, rank_of):
     state = 12345
     keyed = []
     for off in offs:
         state = (state * 1103515245 + 12345) % (1 << 31)
-        keyed.append((-hops(off), state >> 8, off))
-    return [k[2] for k in sorted(keyed)] + [(0, 0, 0, 0)]
-
-
-ORDER = peer_order()
+        keyed.append((rank_of(off), state >> 8, off))
+    return [k[2] for k in sorted(keyed)]
+
+
+EVERY = [
+    (dz, dy, dx, dk)
+    for dz in range(SIDE)
+    for dy in range(SIDE)
+    for dx in range(SIDE)
+    for dk in range(CORES)
+]
+SELF = (0, 0, 0, 0)
+ORDER = shuffled(EVERY[1:], lambda off: 2 in off[:AXES]) + [SELF]
 PEERS = len(ORDER)
+SLOT = {off: i for i, off in enumerate(ORDER)}
+FAR = shuffled(EVERY[1:], lambda off: -hops(off))
+PLANE = [shuffled([o for o in EVERY[1:] if o[a] == 0], lambda off: -hops(off)) + [SELF] for a in range(AXES)]
 GROUP = 8
 CHUNK = 16
 CHUNKS = PEERS // CHUNK
 ROWS = CHUNK * GROUP
+LINE = PEERS // SIDE
 
 
 def kernel(
@@ -74,7 +81,8 @@
     send,
     recv,
     ret,
-    pick,
+    gath,
+    idsg,
     comb,
     prod,
     tails,
@@ -83,6 +91,10 @@
     normed,
     acc,
     lsem,
+    gsend,
+    grecv,
+    isend,
+    irecv,
     dsend,
     drecv,
     rsend,
@@ -120,8 +132,8 @@
     xn = [(x + SIDE - d) % SIDE for d in range(SIDE)]
     ks = [(k + d) % CORES for d in range(CORES)]
 
-    def ahead(i):
-        dz, dy, dx, dk = ORDER[i]
+    def ahead(off):
+        dz, dy, dx, dk = off
         return (zs[dz] + ys[dy] + ks[dk], xs[dx])
 
     def behind(i):
@@ -129,8 +141,8 @@
         return (zn[dz] + yn[dy] + ks[dk], xn[dx])
 
     barrier = pltpu.get_barrier_semaphore()
-    for i in range(PEERS - 1):
-        pl.semaphore_signal(barrier, inc=1, device_id=ahead(i), device_id_type=MESH)
+    for off in FAR:
+        pl.semaphore_signal(barrier, inc=1, device_id=ahead(off), device_id_type=MESH)
 
     mix_in = [
         local(5, gi_hbm, gi),
@@ -164,47 +176,90 @@
     )
 
     tokens = tok.shape[0]
+    width = tok.shape[1]
     sublane = lax.broadcasted_iota(jnp.int32, (GROUP, tokens), 0)
-    off = []
-    for i in range(0, PEERS, GROUP):
-        codes = [dz * 32 + dy * 8 + dk * 4 + dx for dz, dy, dx, dk in ORDER[i : i + GROUP]]
-        part = jnp.full((GROUP, tokens), codes[0], jnp.int32)
-        for j in range(1, GROUP):
-            part = jnp.where(sublane == j, codes[j], part)
-        off.append(part)
-    off = jnp.concatenate(off, axis=0)
-    oz, oy, ok, ox = off // 32, (off // 8) % SIDE, (off // 4) % CORES, off % SIDE
-    target = (
-        (z + oz) % SIDE * 32 + (y + oy) % SIDE * 8 + (k + ok) % CORES * 4 + (x + ox) % SIDE
-    )
-    weights = rw[...]
-    weights = weights / jnp.sum(weights, axis=0, keepdims=True)
-    named = jnp.zeros((PEERS, tokens), jnp.float32)
-    named_weight = jnp.zeros((PEERS, tokens), jnp.float32)
-    for j in range(ids.shape[0]):
-        hit = ids[j : j + 1, :] == target
-        named = jnp.where(hit, 1.0, named)
-        named_weight = jnp.where(hit, weights[j : j + 1, :], named_weight)
     earlier = (
         lax.broadcasted_iota(jnp.int32, (tokens, tokens), 0)
         < lax.broadcasted_iota(jnp.int32, (tokens, tokens), 1)
     ).astype(jnp.bfloat16)
-    rank = jnp.dot(named.astype(jnp.bfloat16), earlier, preferred_element_type=jnp.float32)
-    rank = jnp.where(named > 0.5, rank, 99.0)
-    place = lax.broadcasted_iota(jnp.int32, (PEERS, GROUP, tokens), 1).astype(jnp.float32)
-    chosen = jnp.broadcast_to(rank[:, None, :], (PEERS, GROUP, tokens)) == place
-    pick[...] = (
-        jnp.where(chosen, 1.0, 0.0).reshape(PEERS * GROUP, tokens).astype(jnp.bfloat16)
-    )
-
-    def dispatch(i):
-        rows = pl.ds(i * GROUP, cap)
+    place = lax.broadcasted_iota(jnp.int32, (CHUNK, GROUP, tokens), 1).astype(jnp.float32)
+
+    def experts_at(offs):
+        parts = []
+        for i in range(0, len(offs), GROUP):
+            codes = [dz * 32 + dy * 8 + dk * 4 + dx for dz, dy, dx, dk in offs[i : i + GROUP]]
+            part = jnp.full((GROUP, tokens), codes[0], jnp.int32)
+            for j in range(1, GROUP):
+                part = jnp.where(sublane == j, codes[j], part)
+            parts.append(part)
+        off = jnp.concatenate(parts, axis=0)
+        oz, oy, ok, ox = off // 32, (off // 8) % SIDE, (off // 4) % CORES, off % SIDE
+        return (z + oz) % SIDE * 32 + (y + oy) % SIDE * 8 + (k + ok) % CORES * 4 + (x + ox) % SIDE
+
+    def ranks(named):
+        rank = jnp.dot(named.astype(jnp.bfloat16), earlier, preferred_element_type=jnp.float32)
+        return jnp.where(named > 0.5, rank, 99.0)
+
+    def named_by(listing, target):
+        named = jnp.zeros(target.shape, jnp.float32)
+        for j in range(ids.shape[0]):
+            named = jnp.where(listing[j : j + 1, :] == target, 1.0, named)
+        return named
+
+    lanes = width // 128
+    cuts = [lanes // AXES * p * 128 for p in range(AXES)] + [width]
+
+    def columns(p):
+        return pl.ds(cuts[p], cuts[p + 1] - cuts[p])
+
+    def along(p, d):
+        return tuple(d if a == p else 0 for a in range(AXES)) + (0,)
+
+    def line(p, d):
         return pltpu.make_async_remote_copy(
-            send.at[rows],
-            recv.at[rows],
+            normed.at[:, columns(p)],
+            gath.at[d - 1, :, columns(p)],
+            gsend,
+            grecv.at[p * 4 + d - 1],
+            device_id=ahead(along(p, d)),
+            device_id_type=MESH,
+        )
+
+    def relay(p, d):
+        rows = pl.ds(0 if d == 1 else tokens // 2, tokens // 2)
+        return pltpu.make_async_remote_copy(
+            gath.at[d - 1, rows, columns(p)],
+            gath.at[1, rows, columns(p)],
+            gsend,
+            grecv.at[p * 4 + (1 if d == 1 else 3)],
+            device_id=ahead(along(p, d)),
+            device_id_type=MESH,
+        )
+
+    def listing(p, d):
+        n = p * (SIDE - 1) + d - 1
+        return pltpu.make_async_remote_copy(
+            ids,
+            idsg.at[n],
+            isend.at[n],
+            irecv.at[n],
+            device_id=ahead(along(p, d)),
+            device_id_type=MESH,
+        )
+
+    def dispatch(p, d, i):
+        off = PLANE[p][i]
+        slot = SLOT[tuple(d if a == p else off[a] for a in range(AXES)) + off[AXES:]]
+        source = send.at[pl.ds((d * LINE + i) * GROUP, cap), columns(p)]
+        target = recv.at[pl.ds(slot * GROUP, cap), columns(p)]
+        if off == SELF:
+            return pltpu.make_async_copy(source, target, drecv.at[slot // CHUNK])
+        return pltpu.make_async_remote_copy(
+            source,
+            target,
             dsend,
-            drecv.at[i // CHUNK],
-            device_id=ahead(i),
+            drecv.at[slot // CHUNK],
+            device_id=ahead(off),
             device_id_type=MESH,
         )
 
@@ -226,23 +281,53 @@
         part = ref.at[pl.ds(0, count * GROUP), pl.ds(0, ref.shape[1] * cap // GROUP)]
         return pltpu.make_async_copy(part, part, sem)
 
-    for c in range(CHUNKS):
-        rows = pl.ds(c * ROWS, ROWS)
-        send[rows, :] = jnp.dot(
-            pick[rows, :], normed[...], preferred_element_type=jnp.float32
-        ).astype(jnp.bfloat16)
-        if c == 0:
-            with jax.named_scope("barrier"):
-                pl.semaphore_wait(barrier, PEERS - 1)
-            halo_copy.start()
+    targets = [experts_at(PLANE[p]) for p in range(AXES)]
+    with jax.named_scope("barrier"):
+        pl.semaphore_wait(barrier, PEERS - 1)
+    halo_copy.start()
+    near = (1, SIDE - 1)
+    listings = [listing(p, d) for d in range(1, SIDE) for p in range(AXES)]
+    for copy in listings:
+        copy.start()
+    for d in near:
+        for p in range(AXES):
+            line(p, d).start()
+
+    waiting = []
+
+    def pick_rows(p, d):
+        if d == 0:
+            listed, rows_of = ids[...], normed[:, cuts[p] : cuts[p + 1]]
         else:
-            for i in peers_of(c - 1):
-                dispatch(i).start()
-    for i in peers_of(CHUNKS - 1):
-        dispatch(i).start()
-    own = pl.ds((PEERS - 1) * GROUP, GROUP)
-    recv[own, :] = send[own, :]
-
+            listed = idsg[p * (SIDE - 1) + d - 1]
+            rows_of = gath[d - 1, :, cuts[p] : cuts[p + 1]]
+        rank = ranks(named_by(listed, targets[p]))
+        for h in range(0, LINE, CHUNK):
+            group = jnp.broadcast_to(rank[h : h + CHUNK][:, None, :], place.shape)
+            pick = jnp.where(group == place, 1.0, 0.0).reshape(ROWS, tokens).astype(jnp.bfloat16)
+            send[pl.ds((d * LINE + h) * GROUP, ROWS), cuts[p] : cuts[p + 1]] = jnp.dot(
+                pick, rows_of, preferred_element_type=jnp.float32
+            ).astype(jnp.bfloat16)
+            for copy in waiting:
+                copy.start()
+            waiting[:] = [dispatch(p, d, i) for i in range(h, h + CHUNK)]
+
+    for p in range(AXES):
+        pick_rows(p, 0)
+    with jax.named_scope("listwait"):
+        for copy in listings:
+            copy.wait()
+    for d in near:
+        for p in range(AXES):
+            with jax.named_scope("linewait"):
+                line(p, d).wait_recv()
+            relay(p, d).start()
+    for d in near:
+        for p in range(AXES):
+            pick_rows(p, d)
+    for copy in waiting:
+        copy.start()
+    waiting.clear()
     reach = taps.shape[0] - 1
     for copy in mix_in[:2]:
         copy.wait()
@@ -256,17 +341,6 @@
             .astype(jnp.bfloat16)
             .astype(jnp.float32)
         )
-
-    for c in range(CHUNKS):
-        group = rank[c * CHUNK : (c + 1) * CHUNK]
-        group_weight = named_weight[c * CHUNK : (c + 1) * CHUNK]
-        shape = (CHUNK, GROUP, tokens)
-        share = jnp.where(
-            jnp.broadcast_to(group[:, None, :], shape) == place[:CHUNK],
-            jnp.broadcast_to(group_weight[:, None, :], shape),
-            0.0,
-        ).reshape(ROWS, tokens)
-        comb[c] = share.T.astype(jnp.bfloat16)
 
     for copy in mix_in[2:]:
         copy.wait()
@@ -287,6 +361,14 @@
             gated, wmix[...], preferred_element_type=jnp.float32
         ).astype(jnp.bfloat16)
 
+    for p in range(AXES):
+        with jax.named_scope("relaywait"):
+            for d in near:
+                relay(p, d).wait_recv()
+        pick_rows(p, 2)
+    for copy in waiting:
+        copy.start()
+
     with jax.named_scope('expw_wait'):
         for copy in experts_in:
             copy.wait()
@@ -298,7 +380,7 @@
             @pl.when(c == n)
             def _():
                 with jax.named_scope('dwait'):
-                    all_rows(recv, drecv.at[n], len(peers_of(n))).wait()
+                    all_rows(recv, drecv.at[n], CHUNK).wait()
 
         rows = pl.ds(pl.multiple_of(c * ROWS, ROWS), ROWS)
         block_rows = recv[rows, :]
@@ -330,7 +412,28 @@
                 for i in peers_of(n):
                     giveback(i).start()
 
+    own = pl.ds((PEERS - 1) * GROUP, GROUP)
     ret[own, :] = recv[own, :]
+
+    weights = rw[...]
+    weights = weights / jnp.sum(weights, axis=0, keepdims=True)
+    target = experts_at(ORDER)
+    rank = ranks(named_by(ids[...], target))
+    named_weight = jnp.zeros(target.shape, jnp.float32)
+    for j in range(ids.shape[0]):
+        named_weight = jnp.where(ids[j : j + 1, :] == target, weights[j : j + 1, :], named_weight)
+
+    for c in range(CHUNKS):
+        group = rank[c * CHUNK : (c + 1) * CHUNK]
+        group_weight = named_weight[c * CHUNK : (c + 1) * CHUNK]
+        shape = (CHUNK, GROUP, tokens)
+        share = jnp.where(
+            jnp.broadcast_to(group[:, None, :], shape) == place,
+            jnp.broadcast_to(group_weight[:, None, :], shape),
+            0.0,
+        ).reshape(ROWS, tokens)
+        comb[c] = share.T.astype(jnp.bfloat16)
+
 
     acc[...] = jnp.zeros_like(acc)
     used = lax.broadcasted_iota(jnp.int32, (ROWS, ret.shape[1]), 0) % GROUP < cap
@@ -350,7 +453,8 @@
 
     moe[...] = acc[...].astype(jnp.bfloat16)
     with jax.named_scope('endwait'):
-        all_rows(send, dsend, PEERS - 1).wait()
+        all_rows(send, dsend, SIDE * (LINE - 1)).wait()
+        pltpu.make_async_copy(gath, gath, gsend).wait()
         all_rows(recv, rsend, PEERS - 1).wait()
 
 
@@ -400,7 +504,8 @@
             pltpu.VMEM(slots, bf16),
             pltpu.VMEM(slots, bf16),
             pltpu.VMEM(slots, bf16),
-            pltpu.VMEM((PEERS * GROUP, tokens), bf16),
+            pltpu.VMEM((SIDE - 1, tokens, width), bf16),
+            pltpu.VMEM((AXES * (SIDE - 1), choices, tokens), jnp.int32),
             pltpu.VMEM((CHUNKS, tokens, ROWS), bf16),
             pltpu.VMEM((8 + positions, channels), f32),
             pltpu.VMEM((2, 16, channels), bf16),
@@ -409,6 +514,10 @@
             pltpu.VMEM((tokens, width), bf16),
             pltpu.VMEM((tokens, width), f32),
             pltpu.SemaphoreType.DMA((14,)),
+            pltpu.SemaphoreType.DMA,
+            pltpu.SemaphoreType.DMA((4 * AXES,)),
+            pltpu.SemaphoreType.DMA((AXES * (SIDE - 1),)),
+            pltpu.SemaphoreType.DMA((AXES * (SIDE - 1),)),
             pltpu.SemaphoreType.DMA,
             pltpu.SemaphoreType.DMA((CHUNKS,)),
             pltpu.SemaphoreType.DMA,

time: 86 us -> 82.4 us (0.958)
  Pallas kernels: 82.9 us -> 79.5 us
    pallas_call x1, Pallas kernels: 82.9 us -> 79.5 us  [shards(): pl.pallas_call(functools.partial(kernel, cap), out_shape=(pltpu.VMEM((pos...]
where the time goes in v3:
time: 82.4 us; the launch traced here: 82.3 us
  Pallas kernels  79.5 us (96%)
  local copies, waits for them, and re-layouts  2.11 us (3%)
    pallas_call x1, Pallas kernels, shards(): pl.pallas_call(functools.partial(kernel, cap), out_shape=(pltpu.VMEM((pos...  79.5 us
    unnamed x2, local copies, waits for them, and re-layouts  2.11 us

profile of v3, /device:TPU:1, one launch (start us, length us, event | category | flops | bytes accessed | tf_op | source)
XLA Modules:
  0.0 82.3 jit_solution(9567625806921601800)
XLA Ops:
  0.6 79.5 %layer_step.1 = (bf16[512,2048]{1,0:T(8,128)(2,1)S(1)}, bf16[128,2048]{1,0:T(8,128)(2,1)S(1)}) custom-call(bf16[512,1024]{1,0:T(8,128)(2,1)} %go_hbm.1, bf16[512,1024]{1,0:T(8,128)(2,1)} %gi_hbm.1, bf16[512,1024]{1,0:T(8,128)(2,1)} %ci_hbm.1, f32[3,1024]{1,0:T(4,128)} %taps_hbm.1, bf16[1024,2048]{1,0:T(8,128)(2,1)} %wmix_hbm.1, bf16[128,2048]{1,0:T(8,128)(2,1)} %tok_hbm.1, ...), custom_call_target="tpu_custom_call" | custom-call | tf_op jit(solution)/shard_map/layer_step/pallas_call | solution.py:483
  80.2 1.3 %copy.16 = bf16[512,2048]{1,0:T(8,128)(2,1)} copy(bf16[512,2048]{1,0:T(8,128)(2,1)S(1)} %get-tuple-element.2) | data formatting | bytes 4194304
  81.5 0.8 copy.17

commit v4 on v3

--- a/solution.py
+++ b/solution.py
@@ -38,14 +38,16 @@
     for dk in range(CORES)
 ]
 SELF = (0, 0, 0, 0)
-ORDER = shuffled(EVERY[1:], lambda off: 2 in off[:AXES]) + [SELF]
+BLOCKS = (2, 1, 3)
+ORDER = shuffled(EVERY, lambda off: (off == SELF, 2 in off[:AXES]))
 PEERS = len(ORDER)
 SLOT = {off: i for i, off in enumerate(ORDER)}
 FAR = shuffled(EVERY[1:], lambda off: -hops(off))
 PLANE = [shuffled([o for o in EVERY[1:] if o[a] == 0], lambda off: -hops(off)) + [SELF] for a in range(AXES)]
 GROUP = 8
 CHUNK = 16
-CHUNKS = PEERS // CHUNK
+TILE = 16
+TILES = PEERS // TILE
 ROWS = CHUNK * GROUP
 LINE = PEERS // SIDE
 
@@ -82,7 +84,12 @@
     recv,
     ret,
     gath,
-    idsg,
+    facts,
+    factg,
+    ranked,
+    shared,
+    part,
+    back,
     comb,
     prod,
     tails,
@@ -99,6 +106,8 @@
     drecv,
     rsend,
     rrecv,
+    bsend,
+    brecv,
     hsem,
 ):
     ep = lax.axis_index("ep")
@@ -136,8 +145,8 @@
         dz, dy, dx, dk = off
         return (zs[dz] + ys[dy] + ks[dk], xs[dx])
 
-    def behind(i):
-        dz, dy, dx, dk = ORDER[i]
+    def behind(off):
+        dz, dy, dx, dk = off
         return (zn[dz] + yn[dy] + ks[dk], xn[dx])
 
     barrier = pltpu.get_barrier_semaphore()
@@ -200,12 +209,6 @@
         rank = jnp.dot(named.astype(jnp.bfloat16), earlier, preferred_element_type=jnp.float32)
         return jnp.where(named > 0.5, rank, 99.0)
 
-    def named_by(listing, target):
-        named = jnp.zeros(target.shape, jnp.float32)
-        for j in range(ids.shape[0]):
-            named = jnp.where(listing[j : j + 1, :] == target, 1.0, named)
-        return named
-
     lanes = width // 128
     cuts = [lanes // AXES * p * 128 for p in range(AXES)] + [width]
 
@@ -239,8 +242,8 @@
     def listing(p, d):
         n = p * (SIDE - 1) + d - 1
         return pltpu.make_async_remote_copy(
-            ids,
-            idsg.at[n],
+            facts,
+            factg.at[n],
             isend.at[n],
             irecv.at[n],
             device_id=ahead(along(p, d)),
@@ -253,35 +256,53 @@
         source = send.at[pl.ds((d * LINE + i) * GROUP, cap), columns(p)]
         target = recv.at[pl.ds(slot * GROUP, cap), columns(p)]
         if off == SELF:
-            return pltpu.make_async_copy(source, target, drecv.at[slot // CHUNK])
+            return pltpu.make_async_copy(source, target, drecv.at[slot // TILE])
         return pltpu.make_async_remote_copy(
             source,
             target,
             dsend,
-            drecv.at[slot // CHUNK],
+            drecv.at[slot // TILE],
             device_id=ahead(off),
             device_id_type=MESH,
         )
 
-    def giveback(i):
-        rows = pl.ds(i * GROUP, cap)
+    def giveback(p, slot):
+        off = ORDER[slot]
+        d = off[p]
+        flat = tuple(0 if a == p else off[a] for a in range(AXES)) + off[AXES:]
+        group = d * LINE + PLANE[p].index(flat)
+        source = recv.at[pl.ds(slot * GROUP, cap), columns(p)]
+        target = ret.at[pl.ds(group * GROUP, cap), columns(p)]
+        if flat == SELF:
+            return pltpu.make_async_copy(source, target, rrecv.at[p * SIDE + d])
         return pltpu.make_async_remote_copy(
-            recv.at[rows],
-            ret.at[rows],
+            source,
+            target,
             rsend,
-            rrecv.at[i // CHUNK],
-            device_id=behind(i),
+            rrecv.at[p * SIDE + d],
+            device_id=behind(flat),
             device_id_type=MESH,
         )
 
-    def peers_of(c):
-        return range(c * CHUNK, min((c + 1) * CHUNK, PEERS - 1))
+    def partial(p, d):
+        return pltpu.make_async_remote_copy(
+            part.at[d - 1, :, columns(p)],
+            back.at[d - 1, :, columns(p)],
+            bsend,
+            brecv.at[p * (SIDE - 1) + d - 1],
+            device_id=behind(along(p, d)),
+            device_id_type=MESH,
+        )
 
     def all_rows(ref, sem, count):
         part = ref.at[pl.ds(0, count * GROUP), pl.ds(0, ref.shape[1] * cap // GROUP)]
         return pltpu.make_async_copy(part, part, sem)
 
-    targets = [experts_at(PLANE[p]) for p in range(AXES)]
+    choices = ids.shape[0]
+    weights = rw[...]
+    facts[0:choices, :] = ids[...].astype(jnp.float32)
+    facts[choices:, :] = weights / jnp.sum(weights, axis=0, keepdims=True)
+    targets = [experts_at(PLANE[p]).astype(jnp.float32) for p in range(AXES)]
     with jax.named_scope("barrier"):
         pl.semaphore_wait(barrier, PEERS - 1)
     halo_copy.start()
@@ -297,11 +318,19 @@
 
     def pick_rows(p, d):
         if d == 0:
-            listed, rows_of = ids[...], normed[:, cuts[p] : cuts[p + 1]]
+            known, rows_of = facts[...], normed[:, cuts[p] : cuts[p + 1]]
         else:
-            listed = idsg[p * (SIDE - 1) + d - 1]
+            known = factg[p * (SIDE - 1) + d - 1]
             rows_of = gath[d - 1, :, cuts[p] : cuts[p + 1]]
-        rank = ranks(named_by(listed, targets[p]))
+        named = jnp.zeros(targets[p].shape, jnp.float32)
+        share = jnp.zeros(targets[p].shape, jnp.float32)
+        for j in range(choices):
+            hit = known[j : j + 1, :] == targets[p]
+            named = jnp.where(hit, 1.0, named)
+            share = jnp.where(hit, known[choices + j : choices + j + 1, :], share)
+        rank = ranks(named)
+        ranked[p * SIDE + d] = rank
+        shared[p * SIDE + d] = share
         for h in range(0, LINE, CHUNK):
             group = jnp.broadcast_to(rank[h : h + CHUNK][:, None, :], place.shape)
             pick = jnp.where(group == place, 1.0, 0.0).reshape(ROWS, tokens).astype(jnp.bfloat16)
@@ -369,20 +398,33 @@
     for copy in waiting:
         copy.start()
 
+    @pl.loop(0, AXES * SIDE)
+    def _(n):
+        rank = ranked[n]
+        share = shared[n]
+        for h in range(0, LINE, CHUNK):
+            mine = jnp.broadcast_to(rank[h : h + CHUNK][:, None, :], place.shape) == place
+            mine = jnp.where(
+                mine, jnp.broadcast_to(share[h : h + CHUNK][:, None, :], place.shape), 0.0
+            )
+            comb[n, :, h * GROUP : h * GROUP + ROWS] = mine.reshape(ROWS, tokens).T.astype(
+                jnp.bfloat16
+            )
+
     with jax.named_scope('expw_wait'):
         for copy in experts_in:
             copy.wait()
 
-    @pl.loop(0, CHUNKS)
+    @pl.loop(0, TILES)
     def _(c):
-        for n in range(CHUNKS):
+        for n in range(TILES):
 
             @pl.when(c == n)
             def _():
                 with jax.named_scope('dwait'):
-                    all_rows(recv, drecv.at[n], CHUNK).wait()
-
-        rows = pl.ds(pl.multiple_of(c * ROWS, ROWS), ROWS)
+                    all_rows(recv, drecv.at[n], TILE).wait()
+
+        rows = pl.ds(pl.multiple_of(c * TILE * GROUP, TILE * GROUP), TILE * GROUP)
         block_rows = recv[rows, :]
         hidden = []
         width = 256
@@ -405,57 +447,62 @@
             recv[rows, n : n + width] = jnp.dot(
                 hidden, wd[:, n : n + width], preferred_element_type=jnp.float32
             ).astype(jnp.bfloat16)
-        for n in range(CHUNKS):
+        for n in range(TILES):
 
             @pl.when(c == n)
             def _():
-                for i in peers_of(n):
-                    giveback(i).start()
-
-    own = pl.ds((PEERS - 1) * GROUP, GROUP)
-    ret[own, :] = recv[own, :]
-
-    weights = rw[...]
-    weights = weights / jnp.sum(weights, axis=0, keepdims=True)
-    target = experts_at(ORDER)
-    rank = ranks(named_by(ids[...], target))
-    named_weight = jnp.zeros(target.shape, jnp.float32)
-    for j in range(ids.shape[0]):
-        named_weight = jnp.where(ids[j : j + 1, :] == target, weights[j : j + 1, :], named_weight)
-
-    for c in range(CHUNKS):
-        group = rank[c * CHUNK : (c + 1) * CHUNK]
-        group_weight = named_weight[c * CHUNK : (c + 1) * CHUNK]
-        shape = (CHUNK, GROUP, tokens)
-        share = jnp.where(
-            jnp.broadcast_to(group[:, None, :], shape) == place,
-            jnp.broadcast_to(group_weight[:, None, :], shape),
-            0.0,
-        ).reshape(ROWS, tokens)
-        comb[c] = share.T.astype(jnp.bfloat16)
-
-
-    acc[...] = jnp.zeros_like(acc)
-    used = lax.broadcasted_iota(jnp.int32, (ROWS, ret.shape[1]), 0) % GROUP < cap
-
-    @pl.loop(0, CHUNKS)
-    def _(c):
-        for n in range(CHUNKS):
-
-            @pl.when(c == n)
-            def _():
-                with jax.named_scope('rwait'):
-                    all_rows(ret, rrecv.at[n], len(peers_of(n))).wait()
-
-        rows = pl.ds(pl.multiple_of(c * ROWS, ROWS), ROWS)
-        back = jnp.where(used, ret[rows, :].astype(jnp.float32), 0.0).astype(jnp.bfloat16)
-        acc[...] += jnp.dot(comb[c], back, preferred_element_type=jnp.float32)
-
-    moe[...] = acc[...].astype(jnp.bfloat16)
+                for slot in range(n * TILE, (n + 1) * TILE):
+                    for p in range(AXES):
+                        if ORDER[slot][p]:
+                            giveback(p, slot).start()
+
+    for slot in range(PEERS):
+        for p in range(AXES):
+            if not ORDER[slot][p]:
+                giveback(p, slot).start()
+
+    def added(p, d):
+        with jax.named_scope("rwait"):
+            part_rows = ret.at[pl.ds(0, LINE * cap), columns(p)]
+            pltpu.make_async_copy(part_rows, part_rows, rrecv.at[p * SIDE + d]).wait()
+        rows = ret[pl.ds(d * LINE * GROUP, LINE * GROUP), cuts[p] : cuts[p + 1]]
+        used = lax.broadcasted_iota(jnp.int32, rows.shape, 0) % GROUP < cap
+        rows = jnp.where(used, rows.astype(jnp.float32), 0.0).astype(jnp.bfloat16)
+        return jnp.dot(comb[p * SIDE + d], rows, preferred_element_type=jnp.float32)
+
+    for d in BLOCKS:
+        for p in range(AXES):
+            part[d - 1, :, cuts[p] : cuts[p + 1]] = added(p, d).astype(jnp.bfloat16)
+            partial(p, d).start()
+    for p in range(AXES):
+        acc[:, cuts[p] : cuts[p + 1]] = added(p, 0)
+    for p in range(AXES):
+        total = acc[:, cuts[p] : cuts[p + 1]]
+        for d in BLOCKS:
+            with jax.named_scope("bwait"):
+                partial(p, d).wait_recv()
+            total = total + back[d - 1, :, cuts[p] : cuts[p + 1]].astype(jnp.float32)
+        moe[:, cuts[p] : cuts[p + 1]] = total.astype(jnp.bfloat16)
     with jax.named_scope('endwait'):
         all_rows(send, dsend, SIDE * (LINE - 1)).wait()
         pltpu.make_async_copy(gath, gath, gsend).wait()
-        all_rows(recv, rsend, PEERS - 1).wait()
+        all_rows(recv, rsend, SIDE * (LINE - 1)).wait()
+        pltpu.make_async_copy(part, part, bsend).wait()
+
+
+def flush(parts, mixed, moe, mixed_out, moe_out, sem):
+    rows = mixed.shape[0] // parts
+    copies = [
+        pltpu.make_async_copy(
+            mixed.at[pl.ds(i * rows, rows)], mixed_out.at[pl.ds(i * rows, rows)], sem.at[i]
+        )
+        for i in range(parts)
+    ]
+    copies.append(pltpu.make_async_copy(moe, moe_out, sem.at[parts]))
+    for copy in copies:
+        copy.start()
+    for copy in copies:
+        copy.wait()
 
 
 def shards(
@@ -480,7 +527,7 @@
     bf16, f32 = jnp.bfloat16, jnp.float32
     anywhere = pl.BlockSpec(memory_space=pl.ANY)
     slots = (PEERS * GROUP, width)
-    return pl.pallas_call(
+    mixed, moe = pl.pallas_call(
         functools.partial(kernel, cap),
         out_shape=(
             pltpu.VMEM((positions, width), bf16),
@@ -505,8 +552,13 @@
             pltpu.VMEM(slots, bf16),
             pltpu.VMEM(slots, bf16),
             pltpu.VMEM((SIDE - 1, tokens, width), bf16),
-            pltpu.VMEM((AXES * (SIDE - 1), choices, tokens), jnp.int32),
-            pltpu.VMEM((CHUNKS, tokens, ROWS), bf16),
+            pltpu.VMEM((2 * choices, tokens), f32),
+            pltpu.VMEM((AXES * (SIDE - 1), 2 * choices, tokens), f32),
+            pltpu.VMEM((AXES * SIDE, LINE, tokens), f32),
+            pltpu.VMEM((AXES * SIDE, LINE, tokens), f32),
+            pltpu.VMEM((SIDE - 1, tokens, width), bf16),
+            pltpu.VMEM((SIDE - 1, tokens, width), bf16),
+            pltpu.VMEM((AXES * SIDE, tokens, LINE * GROUP), bf16),
             pltpu.VMEM((8 + positions, channels), f32),
             pltpu.VMEM((2, 16, channels), bf16),
             pltpu.VMEM((16, channels), bf16),
@@ -519,9 +571,11 @@
             pltpu.SemaphoreType.DMA((AXES * (SIDE - 1),)),
             pltpu.SemaphoreType.DMA((AXES * (SIDE - 1),)),
             pltpu.SemaphoreType.DMA,
-            pltpu.SemaphoreType.DMA((CHUNKS,)),
+            pltpu.SemaphoreType.DMA((TILES,)),
             pltpu.SemaphoreType.DMA,
-            pltpu.SemaphoreType.DMA((CHUNKS,)),
+            pltpu.SemaphoreType.DMA((AXES * SIDE,)),
+            pltpu.SemaphoreType.DMA,
+            pltpu.SemaphoreType.DMA((AXES * (SIDE - 1),)),
             pltpu.SemaphoreType.DMA((2,)),
         ],
         compiler_params=pltpu.CompilerParams(
@@ -542,6 +596,19 @@
         expert_up.reshape(width, hidden),
         expert_down.reshape(hidden, width),
     )
+    parts = 4
+    return pl.pallas_call(
+        functools.partial(flush, parts),
+        out_shape=(
+            jax.ShapeDtypeStruct(mixed.shape, bf16),
+            jax.ShapeDtypeStruct(moe.shape, bf16),
+        ),
+        in_specs=[pl.BlockSpec(memory_space=pltpu.VMEM)] * 2,
+        out_specs=(anywhere, anywhere),
+        scratch_shapes=[pltpu.SemaphoreType.DMA((parts + 1,))],
+        compiler_params=pltpu.CompilerParams(vmem_limit_bytes=4 * 2**20),
+        name="flush",
+    )(mixed, moe)
 
 
 def solution(mesh):

time: 82.4 us -> 79.5 us (0.965)
  local copies, waits for them, and re-layouts: 2.11 us -> 0 us
  Pallas kernels: 79.5 us -> 78.5 us
    pallas_call x1, Pallas kernels: 79.5 us -> 77 us  [shards(): pl.pallas_call(functools.partial(kernel, cap), out_shape=(pltpu.VMEM((pos...]
    unnamed x2 -> x0, local copies, waits for them, and re-layouts: 2.11 us -> none
    pallas_call x0 -> x1, Pallas kernels: none -> 1.53 us  [shards(): pl.pallas_call(functools.partial(flush, parts), out_shape=(jax.ShapeDtype...]
where the time goes in v4:
time: 79.5 us; the launch traced here: 79.3 us
  Pallas kernels  78.5 us (99%)
  between operations  0.8 us (1%)
    pallas_call x1, Pallas kernels, shards(): pl.pallas_call(functools.partial(kernel, cap), out_shape=(pltpu.VMEM((pos...  77 us

profile of v4, /device:TPU:1, one launch (start us, length us, event | category | flops | bytes accessed | tf_op | source)
XLA Modules:
  0.0 79.3 jit_solution(17676487252079285500)
XLA Ops:
  0.6 77.0 %layer_step.1 = (bf16[512,2048]{1,0:T(8,128)(2,1)S(1)}, bf16[128,2048]{1,0:T(8,128)(2,1)S(1)}) custom-call(bf16[512,1024]{1,0:T(8,128)(2,1)} %go_hbm.1, bf16[512,1024]{1,0:T(8,128)(2,1)} %gi_hbm.1, bf16[512,1024]{1,0:T(8,128)(2,1)} %ci_hbm.1, f32[3,1024]{1,0:T(4,128)} %taps_hbm.1, bf16[1024,2048]{1,0:T(8,128)(2,1)} %wmix_hbm.1, bf16[128,2048]{1,0:T(8,128)(2,1)} %tok_hbm.1, ...), custom_call_target="tpu_custom_call" | custom-call | tf_op jit(solution)/shard_map/layer_step/pallas_call | solution.py:530
  77.7 1.5 %flush.1 = (bf16[512,2048]{1,0:T(8,128)(2,1)}, bf16[128,2048]{1,0:T(8,128)(2,1)}) custom-call(bf16[512,2048]{1,0:T(8,128)(2,1)S(1)} %get-tuple-element.4.mixed, bf16[128,2048]{1,0:T(8,128)(2,1)S(1)} %get-tuple-element.5.moe), custom_call_target="tpu_custom_call" | custom-call | tf_op jit(solution)/shard_map/flush/pallas_call | solution.py:600

commit v5 on v4

--- a/solution.py
+++ b/solution.py
@@ -315,6 +315,7 @@
             line(p, d).start()
 
     waiting = []
+    held = []
 
     def pick_rows(p, d):
         if d == 0:
@@ -339,7 +340,10 @@
             ).astype(jnp.bfloat16)
             for copy in waiting:
                 copy.start()
-            waiting[:] = [dispatch(p, d, i) for i in range(h, h + CHUNK)]
+            waiting.clear()
+            for i in range(h, h + CHUNK):
+                long_way = d in near and 2 in PLANE[p][i][:AXES]
+                (held if long_way else waiting).append(dispatch(p, d, i))
 
     for p in range(AXES):
         pick_rows(p, 0)
@@ -354,7 +358,7 @@
     for d in near:
         for p in range(AXES):
             pick_rows(p, d)
-    for copy in waiting:
+    for copy in waiting + held:
         copy.start()
     waiting.clear()
     reach = taps.shape[0] - 1

time: 79.5 us -> 78.4 us (0.986)
  Pallas kernels: 78.5 us -> 77.5 us
    pallas_call x1, Pallas kernels: 77 us -> 75.9 us  [shards(): pl.pallas_call(functools.partial(kernel, cap), out_shape=(pltpu.VMEM((pos...]
where the time goes in v5:
time: 78.4 us; the launch traced here: 78.3 us
  Pallas kernels  77.5 us (99%)
  between operations  0.8 us (1%)
    pallas_call x1, Pallas kernels, shards(): pl.pallas_call(functools.partial(kernel, cap), out_shape=(pltpu.VMEM((pos...  75.9 us

profile of v5, /device:TPU:1, one launch (start us, length us, event | category | flops | bytes accessed | tf_op | source)
XLA Modules:
  0.0 78.3 jit_solution(4615037748427238890)
XLA Ops:
  0.6 75.9 %layer_step.1 = (bf16[512,2048]{1,0:T(8,128)(2,1)S(1)}, bf16[128,2048]{1,0:T(8,128)(2,1)S(1)}) custom-call(bf16[512,1024]{1,0:T(8,128)(2,1)} %go_hbm.1, bf16[512,1024]{1,0:T(8,128)(2,1)} %gi_hbm.1, bf16[512,1024]{1,0:T(8,128)(2,1)} %ci_hbm.1, f32[3,1024]{1,0:T(4,128)} %taps_hbm.1, bf16[1024,2048]{1,0:T(8,128)(2,1)} %wmix_hbm.1, bf16[128,2048]{1,0:T(8,128)(2,1)} %tok_hbm.1, ...), custom_call_target="tpu_custom_call" | custom-call | tf_op jit(solution)/shard_map/layer_step/pallas_call | solution.py:534
  76.6 1.5 %flush.1 = (bf16[512,2048]{1,0:T(8,128)(2,1)}, bf16[128,2048]{1,0:T(8,128)(2,1)}) custom-call(bf16[512,2048]{1,0:T(8,128)(2,1)S(1)} %get-tuple-element.4.mixed, bf16[128,2048]{1,0:T(8,128)(2,1)S(1)} %get-tuple-element.5.moe), custom_call_target="tpu_custom_call" | custom-call | tf_op jit(solution)/shard_map/flush/pallas_call | solution.py:604

commit v6 on v5

--- a/solution.py
+++ b/solution.py
@@ -22,7 +22,7 @@
 
 
 def shuffled(offs, rank_of):
-    state = 12345
+    state = 777
     keyed = []
     for off in offs:
         state = (state * 1103515245 + 12345) % (1 << 31)

time: 78.4 us -> 77.6 us (0.990)
  Pallas kernels: 77.5 us -> 76.7 us
    pallas_call x1, Pallas kernels: 75.9 us -> 75.1 us  [shards(): pl.pallas_call(functools.partial(kernel, cap), out_shape=(pltpu.VMEM((pos...]
where the time goes in v6:
time: 77.6 us; the launch traced here: 77.5 us
  Pallas kernels  76.7 us (99%)
  between operations  0.8 us (1%)
    pallas_call x1, Pallas kernels, shards(): pl.pallas_call(functools.partial(kernel, cap), out_shape=(pltpu.VMEM((pos...  75.1 us

profile of v6, /device:TPU:1, one launch (start us, length us, event | category | flops | bytes accessed | tf_op | source)
XLA Modules:
  0.0 77.5 jit_solution(10161660775391712630)
XLA Ops:
  0.6 75.1 %layer_step.1 = (bf16[512,2048]{1,0:T(8,128)(2,1)S(1)}, bf16[128,2048]{1,0:T(8,128)(2,1)S(1)}) custom-call(bf16[512,1024]{1,0:T(8,128)(2,1)} %go_hbm.1, bf16[512,1024]{1,0:T(8,128)(2,1)} %gi_hbm.1, bf16[512,1024]{1,0:T(8,128)(2,1)} %ci_hbm.1, f32[3,1024]{1,0:T(4,128)} %taps_hbm.1, bf16[1024,2048]{1,0:T(8,128)(2,1)} %wmix_hbm.1, bf16[128,2048]{1,0:T(8,128)(2,1)} %tok_hbm.1, ...), custom_call_target="tpu_custom_call" | custom-call | tf_op jit(solution)/shard_map/layer_step/pallas_call | solution.py:534
  75.8 1.5 %flush.1 = (bf16[512,2048]{1,0:T(8,128)(2,1)}, bf16[128,2048]{1,0:T(8,128)(2,1)}) custom-call(bf16[512,2048]{1,0:T(8,128)(2,1)S(1)} %get-tuple-element.4.mixed, bf16[128,2048]{1,0:T(8,128)(2,1)S(1)} %get-tuple-element.5.moe), custom_call_target="tpu_custom_call" | custom-call | tf_op jit(solution)/shard_map/flush/pallas_call | solution.py:604
